TPU v7x, 512 devices: a whole 4x8x8 slice. The times are simulated.
512 devices in a mesh: sp: 128 (over z, y, core), tp: 4 (over x).
Axes of the slice: x: 4, y: 8, z: 8, core: 2. Of those that a mesh axis runs over, the one named last changes fastest.
Arguments:
- tokens: bfloat16 [16384, 2048], P(('sp', 'tp')), may hold values from -6 to 6
- doc_lengths: int32 [16], replicated, may hold values from 1 to 10240, 16384 in all
- query_down: bfloat16 [2048, 512], replicated, may hold values from -0.125 to 0.125
- latent_down: bfloat16 [2048, 256], replicated, may hold values from -0.125 to 0.125
- rope_down: bfloat16 [2048, 32], replicated, may hold values from -0.125 to 0.125
- query_latent_gain: float32 [512], replicated, may hold values from 0.1 to 1.9
- latent_gain: float32 [256], replicated, may hold values from 0.1 to 1.9
- query_up: bfloat16 [512, 768], P(None, 'tp'), may hold values from -0.25 to 0.25
- key_up: bfloat16 [256, 512], P(None, 'tp'), may hold values from -0.375 to 0.375
- value_up: bfloat16 [256, 512], P(None, 'tp'), may hold values from -0.375 to 0.375
- query_gain: float32 [96], replicated, may hold values from 0.5 to 15
- key_gain: float32 [96], replicated, may hold values from 0.5 to 15
- output_gain: float32 [512], replicated, may hold values from 0.1 to 1.9
- output_weight: bfloat16 [512, 2048], P(None, 'tp'), may hold values from -0.25 to 0.25
Outputs:
- layer_output: bfloat16 [16384, 2048], P('sp', 'tp')
- log_totals: float32 [8, 16384], P('tp', 'sp')
Inputs may be any that keep to these rules, and one draw needn't show every extreme that they name: `doc_lengths`: the lengths sum to 16384; the longest is exactly 10240.
All inputs are finite; a program needn't handle non-finite values.
Results may differ from a plain program's by a relative error of at most 0.019.
The roundings to bfloat16 on the way count: a program that leaves them out, or rounds other values in their place, can miss the bound.
Values may be sent and summed in bfloat16 or wider, within the bound.
No kernel may reach another device: no remote copies, remote signals or barrier semaphores. Data moves between devices by JAX's collectives and lax.ppermute only.
A program may use at most 64 MiB of HBM per device.

v0:
```python
import math

import jax
import jax.numpy as jnp
from jax import lax
from jax.experimental import pallas as pl
from jax.experimental.pallas import tpu as pltpu
from jax.sharding import Mesh, PartitionSpec as P


NOPE = 64
ROPE = 32
VD = 64
HW = NOPE + ROPE
KV = HW + VD
HALF = ROPE // 2

EPS = 1e-06
THETA = 10000.0
NEG = -1e30
START = -1e29
ZS, YS, CS, XS = 8, 8, 2, 4
ROWS = 128
MINE = 32
QBLOCKS = 4
KBLOCKS = 2
ROPE_AT = (QBLOCKS + KBLOCKS) * MINE
STEPS = 4
STEP = 512
QB = 256
KB = 256
TAIL = 8
MSG = VD + TAIL
SCALE = HW ** (-0.5)
SCALE2 = SCALE * math.log2(math.e)

f32 = jnp.float32
bf16 = jnp.bfloat16


def start_kernel(
    tok_hbm, query_hbm, latent_hbm, rope_hbm, query_gain_hbm, latent_gain_hbm, out_ref,
    tok_s, query_s, latent_s, rope_s, query_gain_s, latent_gain_s, sems, query_sem, latent_sem,
):
    def part(i):
        return pl.ds(i * STEP, STEP)

    tok_copy = pltpu.make_async_copy(tok_hbm, tok_s, sems.at[0])
    tok_copy.start()
    copies = []
    for i in range(STEPS):
        pair = (
            pltpu.make_async_copy(query_hbm.at[part(i)], query_s.at[part(i)], query_sem.at[i]),
            pltpu.make_async_copy(latent_hbm.at[part(i)], latent_s.at[part(i)], latent_sem.at[i]),
        )
        for copy in pair:
            copy.start()
        copies.append(pair)
    later = (
        pltpu.make_async_copy(rope_hbm, rope_s, sems.at[1]),
        pltpu.make_async_copy(query_gain_hbm, query_gain_s, sems.at[2]),
        pltpu.make_async_copy(latent_gain_hbm, latent_gain_s, sems.at[3]),
    )
    for copy in later:
        copy.start()
    tok_copy.wait()
    query, latent = None, None
    for i in range(STEPS):
        for copy in copies[i]:
            copy.wait()
        tok = tok_s[:, i * STEP : (i + 1) * STEP]
        q = jnp.dot(tok, query_s[i * STEP : (i + 1) * STEP, :], preferred_element_type=f32)
        k = jnp.dot(tok, latent_s[i * STEP : (i + 1) * STEP, :], preferred_element_type=f32)
        query = q if query is None else query + q
        latent = k if latent is None else latent + k

    for copy in later:
        copy.wait()
    rope = lax.dot_general(
        tok_s[...], rope_s[...], (((1,), (1,)), ((), ())), preferred_element_type=f32
    )

    def normed(value, gain):
        square = jnp.sum(value * value, axis=1, keepdims=True) * (1.0 / value.shape[1])
        return (value * lax.rsqrt(square + EPS) * gain).astype(bf16)

    query = normed(query, query_gain_s[...])
    latent = normed(latent, latent_gain_s[...])
    rope = jnp.concatenate([rope[8 * g : 8 * g + 8] for g in range(MINE // 8)], axis=1)
    rope = rope.astype(bf16)
    for x in range(XS):
        for i in range(QBLOCKS):
            out_ref[x, i * MINE : (i + 1) * MINE, :] = query[:, i * 128 : (i + 1) * 128]
        for i in range(KBLOCKS):
            at = (QBLOCKS + i) * MINE
            out_ref[x, at : at + MINE, :] = latent[:, i * 128 : (i + 1) * 128]
        out_ref[x, ROPE_AT:, :] = rope


def rotated(a, b, cosine, sine):
    return a * cosine - b * sine, b * cosine + a * sine


def proj_kernel(
    in_ref, key_up_ref, value_up_ref, query_up_ref, key_gain_ref, query_gain_ref, cos_ref, sin_ref,
    kv_ref, q_ref,
):
    def rows(first, count):
        return jnp.concatenate(
            [
                jnp.concatenate(
                    [
                        in_ref[x, (first + i) * MINE : (first + i + 1) * MINE, :]
                        for i in range(count)
                    ],
                    axis=1,
                )
                for x in range(XS)
            ],
            axis=0,
        )

    lat = rows(QBLOCKS, KBLOCKS)
    plain = lax.dot_general(
        key_up_ref[...], lat, (((0,), (1,)), ((), ())), preferred_element_type=f32
    )
    value = lax.dot_general(
        value_up_ref[...], lat, (((0,), (1,)), ((), ())), preferred_element_type=f32
    ).astype(bf16)
    raw = lax.dot_general(
        query_up_ref[...], rows(0, QBLOCKS), (((1,), (1,)), ((), ())), preferred_element_type=f32
    )
    shared = jnp.concatenate(
        [
            in_ref[x, ROPE_AT:, :].astype(f32)[:, g * ROPE : (g + 1) * ROPE]
            for x in range(XS)
            for g in range(MINE // 8)
        ],
        axis=0,
    )
    shared = jnp.transpose(jnp.concatenate([shared, jnp.zeros((ROWS, 128 - ROPE), f32)], axis=1))
    shared = shared[:ROPE]
    shared_square = jnp.sum(shared * shared, axis=0, keepdims=True)
    gain = key_gain_ref[...]
    query_gain = query_gain_ref[...]
    cosine, sine = cos_ref[...], sin_ref[...]
    for c in range(CS):
        mine = plain[c * NOPE : (c + 1) * NOPE]
        square = (jnp.sum(mine * mine, axis=0, keepdims=True) + shared_square) * (1.0 / HW)
        scale = lax.rsqrt(square + EPS)
        top = mine * scale * gain[:NOPE]
        low = shared * scale * gain[NOPE:]
        a, b = rotated(low[:HALF], low[HALF:], cosine, sine)
        block = jnp.concatenate([top, a, b], axis=0).astype(bf16)
        for z in range(ZS):
            kv_ref[z * CS + c, :HW, :] = block
            kv_ref[z * CS + c, HW:, :] = value[c * VD : (c + 1) * VD]
    for c in range(CS):
        mine = raw[c * HW : (c + 1) * HW]
        square = jnp.sum(mine * mine, axis=0, keepdims=True) * (1.0 / HW)
        mine = mine * lax.rsqrt(square + EPS) * query_gain
        a, b = rotated(mine[NOPE : NOPE + HALF], mine[NOPE + HALF :], cosine, sine)
        q_ref[c * HW : (c + 1) * HW, :] = jnp.concatenate([mine[:NOPE], a, b], axis=0).astype(bf16)


def split_rows(value, width):
    high = value.astype(bf16).astype(f32)
    rest = value - high
    middle = rest.astype(bf16).astype(f32)
    low = rest - middle
    row = lax.broadcasted_iota(jnp.int32, (TAIL, width), 0)
    zero = jnp.zeros((TAIL, width), f32)
    both = jnp.where(row == 0, high, jnp.where(row == 1, middle, jnp.where(row == 2, low, zero)))
    return both.astype(bf16)


def joined_rows(rows):
    rows = rows.astype(f32)
    return (rows[0:1] + rows[1:2]) + rows[2:3]


DOCS = 16
SLAB = 16
AHEAD = 8
PAD = 128 - HW


def ends_of(lengths):
    ends = [lengths[0]]
    for i in range(1, DOCS):
        ends.append(ends[-1] + lengths[i])
    return ends


def doc_of(place, ends):
    doc = (place >= ends[0]).astype(jnp.int32)
    for end in ends[1:]:
        doc = doc + (place >= end).astype(jnp.int32)
    return doc


def attend_kernel(lengths, q_ref, kv_ref, out_ref, k_s, q_s, m_s, l_s, acc_s):
    ends = ends_of(lengths)
    query_base = lax.axis_index("z") * (YS * QB)
    key_base = lax.axis_index("y") * KB
    mine = pl.ds(pl.multiple_of(lax.axis_index("c") * HW, HW), HW)
    row = lax.broadcasted_iota(jnp.int32, (YS, QB), 0)
    lane = lax.broadcasted_iota(jnp.int32, (YS, QB), 1)
    query_doc = doc_of(query_base + row * QB + lane, ends)
    key_doc = doc_of(key_base + row * (YS * QB) + lane, ends)
    index = lax.broadcasted_iota(jnp.int32, (PAD, QB), 0)
    for i in range(ZS * CS):
        half = slice((i % CS) * ROWS, (i % CS + 1) * ROWS)
        same = index[:, half] == key_doc[i // CS : i // CS + 1, half]
        part = jnp.where(same, 1.0, 0.0).astype(bf16)
        k_s[i * ROWS : (i + 1) * ROWS, :] = jnp.transpose(
            jnp.concatenate([kv_ref[i, :HW, :], part], axis=0)
        )
    for i in range(YS):
        q_s[i, :HW, :] = jnp.concatenate(
            [q_ref[2 * i, mine, :], q_ref[2 * i + 1, mine, :]], axis=1
        )
        other = (index != query_doc[i : i + 1]) & (index < DOCS)
        q_s[i, HW:, :] = jnp.where(other, NEG, 0.0).astype(bf16)
    m_s[...] = jnp.full(m_s.shape, START, f32)
    l_s[...] = jnp.zeros(l_s.shape, f32)
    acc_s[...] = jnp.zeros(acc_s.shape, f32)

    first = doc_of(query_base, ends)
    last = doc_of(query_base + (YS * QB - 1), ends)

    def key_step(j, _):
        start = key_base + j * (YS * QB)
        least = doc_of(start, ends)
        most = doc_of(start + (KB - 1), ends)

        @pl.when((least <= last) & (most >= first))
        def _():
            keys = k_s[pl.ds(pl.multiple_of(j * KB, KB), KB), :]
            values = jnp.concatenate([kv_ref[2 * j, HW:, :], kv_ref[2 * j + 1, HW:, :]], axis=1)
            issued = [jnp.dot(keys, q_s[t], preferred_element_type=f32) for t in range(AHEAD)]
            peak = jnp.max(issued[0], axis=0, keepdims=True)
            waiting = None
            for at in range(YS):
                scores = issued[at]
                before = m_s[at]
                now = jnp.maximum(before, peak)
                rescale = jnp.exp2((before - now) * SCALE2)
                m_s[at] = now
                if at + AHEAD < YS:
                    issued.append(jnp.dot(keys, q_s[at + AHEAD], preferred_element_type=f32))
                if at + 1 < YS:
                    ahead = issued[at + 1]
                    peaks = jnp.full((8, QB), START, f32)
                sums = jnp.zeros((8, QB), f32)
                pieces = []
                for r in range(0, KB, SLAB):
                    w = jnp.exp2((scores[r : r + SLAB] - now) * SCALE2)
                    for i in range(0, SLAB, 8):
                        sums = sums + w[i : i + 8]
                    pieces.append(w.astype(bf16))
                    if at + 1 < YS:
                        for i in range(r, r + SLAB, 8):
                            peaks = jnp.maximum(peaks, ahead[i : i + 8])
                if waiting is not None:
                    was, scaled, product = waiting
                    acc_s[was] = acc_s[was] * scaled + product
                product = jnp.dot(
                    values, jnp.concatenate(pieces, axis=0), preferred_element_type=f32
                )
                waiting = (at, rescale, product)
                l_s[at] = l_s[at] * rescale + jnp.sum(sums, axis=0, keepdims=True)
                if at + 1 < YS:
                    peak = jnp.max(peaks, axis=0, keepdims=True)
            was, scaled, product = waiting
            acc_s[was] = acc_s[was] * scaled + product

        return 0

    lax.fori_loop(0, ZS, key_step, 0)
    for i in range(YS):
        total = l_s[i]
        some = total > 0.0
        safe = jnp.where(some, total, 1.0)
        logs = jnp.where(some, m_s[i] * SCALE + jnp.log(safe), NEG)
        out_ref[i, :VD, :] = (acc_s[i] / safe).astype(bf16)
        out_ref[i, VD:, :] = split_rows(logs, QB)


def combine_kernel(in_ref, out_ref):
    logs = [joined_rows(in_ref[i, VD:, :]) for i in range(YS)]
    top = logs[0]
    for v in logs[1:]:
        top = jnp.maximum(top, v)
    total = jnp.zeros((1, QB), f32)
    mixed = jnp.zeros((VD, QB), f32)
    for i in range(YS):
        w = jnp.exp(logs[i] - top)
        total = total + w
        mixed = mixed + w * in_ref[i, :VD, :].astype(f32)
    head = (mixed / total).astype(bf16)
    tail = split_rows(top + jnp.log(total), QB)
    for c in range(CS):
        for x in range(XS):
            out_ref[c * XS + x, :VD, :] = head[:, c * ROWS : (c + 1) * ROWS]
            out_ref[c * XS + x, VD:, :] = tail[:, c * ROWS : (c + 1) * ROWS]


def column_kernel(gain_ref, out_ref):
    gain = gain_ref[...]
    out_ref[...] = jnp.transpose(jnp.broadcast_to(gain, (ROWS, gain.shape[1])))


def output_kernel(x_at, in_ref, first_ref, second_ref, weight_ref, out_ref, log_ref):
    heads = []
    for x in range(XS):
        for c in range(CS):
            heads.append(in_ref[c * XS + x, :VD, :].astype(f32))
    joined = jnp.concatenate(heads, axis=0)
    square = jnp.sum(joined * joined, axis=0, keepdims=True) * (1.0 / joined.shape[0])
    gain = jnp.concatenate([first_ref[...], second_ref[...]], axis=0)
    normed = (joined * lax.rsqrt(square + EPS) * gain).astype(bf16)
    out_ref[...] = lax.dot_general(
        normed, weight_ref[...], (((0,), (0,)), ((), ())), preferred_element_type=f32
    ).astype(bf16)
    for c in range(CS):
        log_ref[c : c + 1, :] = joined_rows(in_ref[c * XS + x_at[0], VD:, :])


def smem():
    return pl.BlockSpec(memory_space=pltpu.SMEM)


def hbm():
    return pl.BlockSpec(memory_space=pltpu.HBM)


def vmem():
    return pl.BlockSpec(memory_space=pltpu.VMEM)


def call(kernel, out_shape, scalars, arrays, scratch=()):
    many = isinstance(out_shape, (tuple, list))
    return pl.pallas_call(
        kernel,
        out_shape=out_shape,
        in_specs=[smem()] * len(scalars) + [vmem()] * len(arrays),
        out_specs=[vmem() for _ in out_shape] if many else vmem(),
        scratch_shapes=list(scratch),
        compiler_params=pltpu.CompilerParams(vmem_limit_bytes=32 * 1024 * 1024),
    )(*scalars, *arrays)


def run_attend(doc_lengths, q_all, kv_all):
    return call(
        attend_kernel,
        jax.ShapeDtypeStruct((YS, MSG, QB), bf16),
        (doc_lengths,),
        (q_all, kv_all),
        scratch=(
            pltpu.VMEM((ZS * KB, 128), bf16),
            pltpu.VMEM((YS, 128, QB), bf16),
            pltpu.VMEM((YS, 1, QB), f32),
            pltpu.VMEM((YS, 1, QB), f32),
            pltpu.VMEM((YS, VD, QB), f32),
        ),
    )


def per_device(
    tokens,
    doc_lengths,
    query_down,
    latent_down,
    rope_down,
    query_latent_gain,
    latent_gain,
    query_up,
    key_up,
    value_up,
    query_gain,
    key_gain,
    output_gain,
    output_weight,
):
    z_at, y_at, c_at, x_at = (lax.axis_index(a) for a in ("z", "y", "c", "x"))
    packed = pl.pallas_call(
        start_kernel,
        out_shape=jax.ShapeDtypeStruct((XS, ROPE_AT + 8, 128), bf16),
        in_specs=[hbm()] * 6,
        out_specs=vmem(),
        scratch_shapes=[
            pltpu.VMEM(tokens.shape, bf16),
            pltpu.VMEM(query_down.shape, bf16),
            pltpu.VMEM(latent_down.shape, bf16),
            pltpu.VMEM(rope_down.shape[::-1], bf16),
            pltpu.VMEM((1, *query_latent_gain.shape), f32),
            pltpu.VMEM((1, *latent_gain.shape), f32),
            pltpu.SemaphoreType.DMA((4,)),
            pltpu.SemaphoreType.DMA((STEPS,)),
            pltpu.SemaphoreType.DMA((STEPS,)),
        ],
        compiler_params=pltpu.CompilerParams(vmem_limit_bytes=63 * 1024 * 1024),
        name="start",
    )(
        tokens,
        query_down,
        latent_down,
        rope_down.T,
        query_latent_gain.reshape(1, -1),
        latent_gain.reshape(1, -1),
    )
    every = lax.all_to_all(packed, "x", split_axis=0, concat_axis=0, tiled=True)

    offset = ((z_at * YS + y_at) * CS + c_at) * ROWS
    places = offset + jnp.arange(ROWS, dtype=jnp.int32)
    inverse = THETA ** (-jnp.arange(HALF, dtype=f32) / HALF)
    angles = places.astype(f32)[None, :] * inverse[:, None]
    cosine, sine = jnp.cos(angles), jnp.sin(angles)

    kv_out, q_out = call(
        proj_kernel,
        (
            jax.ShapeDtypeStruct((ZS * CS, KV, ROWS), bf16),
            jax.ShapeDtypeStruct((CS * HW, ROWS), bf16),
        ),
        (),
        (
            every,
            key_up,
            value_up,
            query_up.T,
            key_gain[:, None],
            query_gain[:, None],
            cosine,
            sine,
        ),
    )
    kv_all = lax.all_to_all(kv_out, ("z", "c"), split_axis=0, concat_axis=0, tiled=True)
    q_all = lax.all_gather(q_out, ("y", "c"), axis=0)

    parts = run_attend(doc_lengths, q_all, kv_all)
    parts = lax.all_to_all(parts, "y", split_axis=0, concat_axis=0, tiled=True)
    half = output_gain.shape[0] // 2
    column = jax.ShapeDtypeStruct((half, ROWS), f32)
    first = call(column_kernel, column, (), (output_gain[:half].reshape(1, -1),))
    second = call(column_kernel, column, (), (output_gain[half:].reshape(1, -1),))
    heads = call(combine_kernel, jax.ShapeDtypeStruct((CS * XS, MSG, ROWS), bf16), (), (parts,))
    heads = lax.all_to_all(heads, ("c", "x"), split_axis=0, concat_axis=0, tiled=True)
    layer_output, log_totals = call(
        output_kernel,
        (
            jax.ShapeDtypeStruct((ROWS, output_weight.shape[1]), bf16),
            jax.ShapeDtypeStruct((CS, ROWS), f32),
        ),
        (x_at.astype(jnp.int32).reshape(1),),
        (heads, first, second, output_weight),
    )
    return (layer_output, log_totals)


def solution(mesh):
    fine = Mesh(mesh.devices.reshape(ZS, YS, CS, XS), ("z", "y", "c", "x"))
    sp = ("z", "y", "c")

    return jax.shard_map(
        per_device,
        mesh=fine,
        in_specs=(
            P((*sp, "x"), None),
            P(),
            P(),
            P(),
            P(),
            P(),
            P(),
            P(None, "x"),
            P(None, "x"),
            P(None, "x"),
            P(),
            P(),
            P(),
            P(None, "x"),
        ),
        out_specs=(P(sp, "x"), P("x", sp)),
        check_vma=False,
    )
```

profile of v0, /device:TPU:1, one launch (start us, length us, event | category | flops | bytes accessed | tf_op | source)
XLA Modules:
  0.0 83.9 jit_solution(970492188638183596)
XLA Ops:
  0.6 0.0 copy-start.6
  0.6 0.0 copy-start.7
  0.7 0.0 copy-start.3
  0.7 0.0 copy-start.2
  0.7 0.0 copy-start.1
  0.7 3.3 %start.1 = bf16[4,200,128]{2,1,0:T(8,128)(2,1)} custom-call(bf16[32,2048]{1,0:T(8,128)(2,1)} %tok_hbm.1, bf16[2048,512]{1,0:T(8,128)(2,1)} %query_hbm.1, bf16[2048,256]{1,0:T(8,128)(2,1)} %latent_hbm.1, bf16[32,2048]{1,0:T(8,128)(2,1)} %bitcast.14, f32[1,512]{1,0:T(1,128)} %bitcast.15, f32[1,256]{1,0:T(1,128)} %bitcast.16), custom_call_target="tpu_custom_call" | custom-call | tf_op jit(solution)/shard_map/start/pallas_call | solution.py:387
  4.0 0.0 copy-start.4
  4.0 4.8 %all-to-all-start = ((bf16[4,200,128]{2,1,0:T(8,128)(2,1)}), bf16[4,200,128]{2,1,0:T(8,128)(2,1)S(1)}, u32[]{:S(2)}, u32[]{:S(2)}) async-start(bf16[4,200,128]{2,1,0:T(8,128)(2,1)} %start.1), calls=%async_computation | async-start | bytes 409600 | tf_op jit(solution)/shard_map/all_to_all | solution.py:413
  8.9 0.0 copy-done.6
  8.9 0.1 copy.17.query_gain_ref
  9.0 0.0 copy-done.7
  9.0 0.1 copy.16.key_gain_ref
  9.1 0.1 multiply_sine_fusion
  9.2 4.8 %all-to-all-done.in_ref = bf16[4,200,128]{2,1,0:T(8,128)(2,1)S(1)} async-done(((bf16[4,200,128]{2,1,0:T(8,128)(2,1)}), bf16[4,200,128]{2,1,0:T(8,128)(2,1)S(1)}, u32[]{:S(2)}, u32[]{:S(2)}) %all-to-all-start) | async-done | bytes 204832 | tf_op jit(solution)/shard_map/all_to_all | solution.py:413
  14.1 0.0 copy-done.3
  14.1 0.0 copy-done.2
  14.1 0.0 copy-done.1
  14.1 1.1 %shard_map.149 = (bf16[16,160,128]{2,1,0:T(8,128)(2,1)}, bf16[192,128]{1,0:T(8,128)(2,1)S(1)}) custom-call(bf16[4,200,128]{2,1,0:T(8,128)(2,1)S(1)} %all-to-all-done.in_ref, bf16[256,128]{1,0:T(8,128)(2,1)S(1)} %copy-done.2, bf16[256,128]{1,0:T(8,128)(2,1)S(1)} %copy-done.3, bf16[192,512]{1,0:T(8,128)(2,1)S(1)} %bitcast.11, f32[96,1]{1,0:T(8,128)S(1)} %copy.16.key_gain_ref, ...), custom_call_target="tpu_custom_call" | custom-call | tf_op jit(solution)/shard_map/pallas_call | solution.py:344
  15.2 12.4 %all-to-all-start.1 = ((bf16[16,160,128]{2,1,0:T(8,128)(2,1)}), bf16[16,160,128]{2,1,0:T(8,128)(2,1)S(1)}, u32[]{:S(2)}, u32[]{:S(2)}) async-start(bf16[16,160,128]{2,1,0:T(8,128)(2,1)} %get-tuple-element.5), calls=%async_computation.1 | async-start | bytes 1310720 | tf_op jit(solution)/shard_map/all_to_all | solution.py:439
  27.7 0.0 copy-start.5
  27.7 0.0 copy-start
  27.7 19.8 %all-gather = bf16[3072,128]{1,0:T(8,128)(2,1)S(1)} all-gather(bf16[192,128]{1,0:T(8,128)(2,1)S(1)} %get-tuple-element.4), channel_id=2, replica_groups=mesh['z'=8,'y'=8,'c'=2,'x'=4] {'y','c'}, dimensions={0}, use_global_device_ids=true | all-gather | bytes 835584 | tf_op jit(solution)/shard_map/all_gather | solution.py:440
  47.5 0.1 all-to-all-done.1.kv_ref
  47.6 0.0 copy-done.4
  47.6 7.3 %shard_map.150 = bf16[8,72,256]{2,1,0:T(8,128)(2,1)} custom-call(s32[16]{0:T(128)S(1)} %copy-done.4, bf16[16,192,128]{2,1,0:T(8,128)(2,1)S(1)} %bitcast.10, bf16[16,160,128]{2,1,0:T(8,128)(2,1)S(1)} %all-to-all-done.1.kv_ref), custom_call_target="tpu_custom_call" | custom-call | tf_op jit(solution)/shard_map/pallas_call | solution.py:344
  54.9 6.8 %all-to-all-start.2 = ((bf16[8,72,256]{2,1,0:T(8,128)(2,1)}), bf16[8,72,256]{2,1,0:T(8,128)(2,1)S(1)}, u32[]{:S(2)}, u32[]{:S(2)}) async-start(bf16[8,72,256]{2,1,0:T(8,128)(2,1)} %shard_map.150), calls=%async_computation.2 | async-start | bytes 589824 | tf_op jit(solution)/shard_map/all_to_all | solution.py:443
  61.7 12.0 %all-to-all-done.2.in_ref = bf16[8,72,256]{2,1,0:T(8,128)(2,1)S(1)} async-done(((bf16[8,72,256]{2,1,0:T(8,128)(2,1)}), bf16[8,72,256]{2,1,0:T(8,128)(2,1)S(1)}, u32[]{:S(2)}, u32[]{:S(2)}) %all-to-all-start.2) | async-done | bytes 294944 | tf_op jit(solution)/shard_map/all_to_all | solution.py:443
  73.7 0.8 shard_map.151
  74.5 3.3 %all-to-all-start.3 = ((bf16[8,72,128]{2,1,0:T(8,128)(2,1)}), bf16[8,72,128]{2,1,0:T(8,128)(2,1)S(1)}, u32[]{:S(2)}, u32[]{:S(2)}) async-start(bf16[8,72,128]{2,1,0:T(8,128)(2,1)} %shard_map.151), calls=%async_computation.3 | async-start | bytes 294912 | tf_op jit(solution)/shard_map/all_to_all | solution.py:449
  77.8 0.0 copy-done.5
  77.9 0.1 shard_map.152.first_ref
  78.0 0.1 shard_map.153.second_ref
  78.1 4.9 %all-to-all-done.3.in_ref = bf16[8,72,128]{2,1,0:T(8,128)(2,1)S(1)} async-done(((bf16[8,72,128]{2,1,0:T(8,128)(2,1)}), bf16[8,72,128]{2,1,0:T(8,128)(2,1)S(1)}, u32[]{:S(2)}, u32[]{:S(2)}) %all-to-all-start.3) | async-done | bytes 147488 | tf_op jit(solution)/shard_map/all_to_all | solution.py:449
  82.9 0.0 copy-done
  82.9 1.0 %shard_map.154 = (bf16[128,512]{1,0:T(8,128)(2,1)}, f32[2,128]{1,0:T(2,128)}) custom-call(s32[1]{0:T(128)} %bitcast.x_at, bf16[8,72,128]{2,1,0:T(8,128)(2,1)S(1)} %all-to-all-done.3.in_ref, f32[256,128]{1,0:T(8,128)S(1)} %shard_map.152.first_ref, f32[256,128]{1,0:T(8,128)S(1)} %shard_map.153.second_ref, bf16[512,512]{1,0:T(8,128)(2,1)S(1)} %copy-done), custom_call_target="tpu_custom_call" | custom-call | tf_op jit(solution)/shard_map/pallas_call | solution.py:344
  (3 shorter events, 0.0 us)
Async XLA Ops:
  0.6 8.3 %copy-start.6 = (f32[96]{0:T(128)S(1)}, f32[96]{0:T(128)}, u32[]{:S(2)}) copy-start(f32[96]{0:T(128)} %param.24) | copy-start | bytes 1156
  0.6 8.4 %copy-start.7 = (f32[96]{0:T(128)S(1)}, f32[96]{0:T(128)}, u32[]{:S(2)}) copy-start(f32[96]{0:T(128)} %param.25) | copy-start | bytes 1156
  0.7 13.4 %copy-start.3 = (bf16[256,128]{1,0:T(8,128)(2,1)S(1)}, bf16[256,128]{1,0:T(8,128)(2,1)}, u32[]{:S(2)}) copy-start(bf16[256,128]{1,0:T(8,128)(2,1)} %value_up_ref.1) | copy-start | bytes 196612
  0.7 13.4 %copy-start.2 = (bf16[256,128]{1,0:T(8,128)(2,1)S(1)}, bf16[256,128]{1,0:T(8,128)(2,1)}, u32[]{:S(2)}) copy-start(bf16[256,128]{1,0:T(8,128)(2,1)} %key_up_ref.1) | copy-start | bytes 196612
  0.7 13.4 %copy-start.1 = (bf16[512,192]{0,1:T(8,128)(2,1)S(1)}, bf16[512,192]{0,1:T(8,128)(2,1)}, u32[]{:S(2)}) copy-start(bf16[512,192]{0,1:T(8,128)(2,1)} %param.21) | copy-start | bytes 589828
  4.0 43.6 %copy-start.4 = (s32[16]{0:T(128)S(1)}, s32[16]{0:T(128)}, u32[]{:S(2)}) copy-start(s32[16]{0:T(128)} %lengths.1) | copy-start | bytes 196
  4.0 10.1 %all-to-all-start = ((bf16[4,200,128]{2,1,0:T(8,128)(2,1)}), bf16[4,200,128]{2,1,0:T(8,128)(2,1)S(1)}, u32[]{:S(2)}, u32[]{:S(2)}) async-start(bf16[4,200,128]{2,1,0:T(8,128)(2,1)} %start.1), calls=%async_computation | async-start | bytes 409600 | tf_op jit(solution)/shard_map/all_to_all | solution.py:413
  15.2 32.4 %all-to-all-start.1 = ((bf16[16,160,128]{2,1,0:T(8,128)(2,1)}), bf16[16,160,128]{2,1,0:T(8,128)(2,1)S(1)}, u32[]{:S(2)}, u32[]{:S(2)}) async-start(bf16[16,160,128]{2,1,0:T(8,128)(2,1)} %get-tuple-element.5), calls=%async_computation.1 | async-start | bytes 1310720 | tf_op jit(solution)/shard_map/all_to_all | solution.py:439
  27.7 50.2 %copy-start.5 = (f32[512]{0:T(512)S(1)}, f32[512]{0:T(512)}, u32[]{:S(2)}) copy-start(f32[512]{0:T(512)} %param.26) | copy-start | bytes 6148
  27.7 55.3 %copy-start = (bf16[512,512]{1,0:T(8,128)(2,1)S(1)}, bf16[512,512]{1,0:T(8,128)(2,1)}, u32[]{:S(2)}) copy-start(bf16[512,512]{1,0:T(8,128)(2,1)} %weight_ref.1) | copy-start | bytes 1572868
  54.9 18.8 %all-to-all-start.2 = ((bf16[8,72,256]{2,1,0:T(8,128)(2,1)}), bf16[8,72,256]{2,1,0:T(8,128)(2,1)S(1)}, u32[]{:S(2)}, u32[]{:S(2)}) async-start(bf16[8,72,256]{2,1,0:T(8,128)(2,1)} %shard_map.150), calls=%async_computation.2 | async-start | bytes 589824 | tf_op jit(solution)/shard_map/all_to_all | solution.py:443
  74.5 8.4 %all-to-all-start.3 = ((bf16[8,72,128]{2,1,0:T(8,128)(2,1)}), bf16[8,72,128]{2,1,0:T(8,128)(2,1)S(1)}, u32[]{:S(2)}, u32[]{:S(2)}) async-start(bf16[8,72,128]{2,1,0:T(8,128)(2,1)} %shard_map.151), calls=%async_computation.3 | async-start | bytes 294912 | tf_op jit(solution)/shard_map/all_to_all | solution.py:449
where the time goes:
time: 84.4 us; the launch traced here: 83.9 us
  starting transfers between devices  27.4 us (32%)
  waiting for transfers between devices  21.8 us (26%)
  blocking collectives  19.8 us (23%)
  Pallas kernels  13.7 us (16%)
    all_gather x1, blocking collectives, per_device(): q_all = lax.all_gather(q_out, ('y', 'c'), axis=0)  19.8 us
    all_to_all x1, starting transfers between devices, per_device(): lax.all_to_all(kv_out, ('z', 'c'), split_axis=0, concat_axis=0, tiled=True)  12.4 us
    all_to_all x1, waiting for transfers between devices, per_device(): parts = lax.all_to_all(parts, 'y', split_axis=0, concat_axis=0, tiled=True)  12 us
    pallas_call x6, Pallas kernels, call(): pl.pallas_call(kernel, out_shape=out_shape, in_specs=[smem()] * len(scala...  10.4 us
    all_to_all x1, starting transfers between devices, per_device(): parts = lax.all_to_all(parts, 'y', split_axis=0, concat_axis=0, tiled=True)  6.83 us
    all_to_all x1, waiting for transfers between devices, per_device(): lax.all_to_all(heads, ('c', 'x'), split_axis=0, concat_axis=0, tiled=True)  4.85 us
    all_to_all x1, waiting for transfers between devices, per_device(): every = lax.all_to_all(packed, 'x', split_axis=0, concat_axis=0, tiled=True)  4.85 us
    all_to_all x1, starting transfers between devices, per_device(): every = lax.all_to_all(packed, 'x', split_axis=0, concat_axis=0, tiled=True)  4.84 us
  transfers between devices with their start and end apart: 4, of which 4 were waited for; matrix products, arithmetic and copies ran while one was open for 0% of the time, Pallas kernels for 0%

commit v1 on v0

--- a/solution.py
+++ b/solution.py
@@ -39,14 +39,22 @@
 
 
 def start_kernel(
-    tok_hbm, query_hbm, latent_hbm, rope_hbm, query_gain_hbm, latent_gain_hbm, out_ref,
-    tok_s, query_s, latent_s, rope_s, query_gain_s, latent_gain_s, sems, query_sem, latent_sem,
+    tok_hbm, query_hbm, latent_hbm, rope_hbm, query_gain_hbm, latent_gain_hbm, out_hbm,
+    tok_s, query_s, latent_s, rope_s, query_gain_s, latent_gain_s, out_s,
+    sems, query_sem, latent_sem, out_sem,
 ):
     def part(i):
         return pl.ds(i * STEP, STEP)
 
     tok_copy = pltpu.make_async_copy(tok_hbm, tok_s, sems.at[0])
     tok_copy.start()
+    later = (
+        pltpu.make_async_copy(rope_hbm, rope_s, sems.at[1]),
+        pltpu.make_async_copy(query_gain_hbm, query_gain_s, sems.at[2]),
+        pltpu.make_async_copy(latent_gain_hbm, latent_gain_s, sems.at[3]),
+    )
+    for copy in later:
+        copy.start()
     copies = []
     for i in range(STEPS):
         pair = (
@@ -56,14 +64,12 @@
         for copy in pair:
             copy.start()
         copies.append(pair)
-    later = (
-        pltpu.make_async_copy(rope_hbm, rope_s, sems.at[1]),
-        pltpu.make_async_copy(query_gain_hbm, query_gain_s, sems.at[2]),
-        pltpu.make_async_copy(latent_gain_hbm, latent_gain_s, sems.at[3]),
-    )
+    tok_copy.wait()
     for copy in later:
-        copy.start()
-    tok_copy.wait()
+        copy.wait()
+    rope = lax.dot_general(
+        tok_s[...], rope_s[...], (((1,), (1,)), ((), ())), preferred_element_type=f32
+    )
     query, latent = None, None
     for i in range(STEPS):
         for copy in copies[i]:
@@ -74,11 +80,6 @@
         query = q if query is None else query + q
         latent = k if latent is None else latent + k
 
-    for copy in later:
-        copy.wait()
-    rope = lax.dot_general(
-        tok_s[...], rope_s[...], (((1,), (1,)), ((), ())), preferred_element_type=f32
-    )
 
     def normed(value, gain):
         square = jnp.sum(value * value, axis=1, keepdims=True) * (1.0 / value.shape[1])
@@ -88,13 +89,17 @@
     latent = normed(latent, latent_gain_s[...])
     rope = jnp.concatenate([rope[8 * g : 8 * g + 8] for g in range(MINE // 8)], axis=1)
     rope = rope.astype(bf16)
-    for x in range(XS):
-        for i in range(QBLOCKS):
-            out_ref[x, i * MINE : (i + 1) * MINE, :] = query[:, i * 128 : (i + 1) * 128]
-        for i in range(KBLOCKS):
-            at = (QBLOCKS + i) * MINE
-            out_ref[x, at : at + MINE, :] = latent[:, i * 128 : (i + 1) * 128]
-        out_ref[x, ROPE_AT:, :] = rope
+    for i in range(QBLOCKS):
+        out_s[i * MINE : (i + 1) * MINE, :] = query[:, i * 128 : (i + 1) * 128]
+    for i in range(KBLOCKS):
+        at = (QBLOCKS + i) * MINE
+        out_s[at : at + MINE, :] = latent[:, i * 128 : (i + 1) * 128]
+    out_s[ROPE_AT:, :] = rope
+    copies = [pltpu.make_async_copy(out_s, out_hbm.at[x], out_sem.at[x]) for x in range(XS)]
+    for copy in copies:
+        copy.start()
+    for copy in copies:
+        copy.wait()
 
 
 def rotated(a, b, cosine, sine):
@@ -103,7 +108,7 @@
 
 def proj_kernel(
     in_ref, key_up_ref, value_up_ref, query_up_ref, key_gain_ref, query_gain_ref, cos_ref, sin_ref,
-    kv_ref, q_ref,
+    kv_hbm, q_ref, kv_s, kv_sem,
 ):
     def rows(first, count):
         return jnp.concatenate(
@@ -144,6 +149,7 @@
     gain = key_gain_ref[...]
     query_gain = query_gain_ref[...]
     cosine, sine = cos_ref[...], sin_ref[...]
+    copies = []
     for c in range(CS):
         mine = plain[c * NOPE : (c + 1) * NOPE]
         square = (jnp.sum(mine * mine, axis=0, keepdims=True) + shared_square) * (1.0 / HW)
@@ -151,16 +157,20 @@
         top = mine * scale * gain[:NOPE]
         low = shared * scale * gain[NOPE:]
         a, b = rotated(low[:HALF], low[HALF:], cosine, sine)
-        block = jnp.concatenate([top, a, b], axis=0).astype(bf16)
+        kv_s[c, :HW, :] = jnp.concatenate([top, a, b], axis=0).astype(bf16)
+        kv_s[c, HW:, :] = value[c * VD : (c + 1) * VD]
         for z in range(ZS):
-            kv_ref[z * CS + c, :HW, :] = block
-            kv_ref[z * CS + c, HW:, :] = value[c * VD : (c + 1) * VD]
+            at = z * CS + c
+            copies.append(pltpu.make_async_copy(kv_s.at[c], kv_hbm.at[at], kv_sem.at[at]))
+            copies[-1].start()
     for c in range(CS):
         mine = raw[c * HW : (c + 1) * HW]
         square = jnp.sum(mine * mine, axis=0, keepdims=True) * (1.0 / HW)
         mine = mine * lax.rsqrt(square + EPS) * query_gain
         a, b = rotated(mine[NOPE : NOPE + HALF], mine[NOPE + HALF :], cosine, sine)
         q_ref[c * HW : (c + 1) * HW, :] = jnp.concatenate([mine[:NOPE], a, b], axis=0).astype(bf16)
+    for copy in copies:
+        copy.wait()
 
 
 def split_rows(value, width):
@@ -185,33 +195,35 @@
 PAD = 128 - HW
 
 
-def ends_of(lengths):
-    ends = [lengths[0]]
-    for i in range(1, DOCS):
-        ends.append(ends[-1] + lengths[i])
-    return ends
-
-
-def doc_of(place, ends):
-    doc = (place >= ends[0]).astype(jnp.int32)
-    for end in ends[1:]:
-        doc = doc + (place >= end).astype(jnp.int32)
-    return doc
-
-
-def attend_kernel(lengths, q_ref, kv_ref, out_ref, k_s, q_s, m_s, l_s, acc_s):
-    ends = ends_of(lengths)
+def table_kernel(lengths, query_ref, key_ref):
+    row = lax.broadcasted_iota(jnp.int32, (YS, QB), 0)
+    lane = lax.broadcasted_iota(jnp.int32, (YS, QB), 1)
+    query_place = lax.axis_index("z") * (YS * QB) + row * QB + lane
+    key_place = lax.axis_index("y") * KB + row * (YS * QB) + lane
+    end = jnp.int32(0)
+    query_doc = jnp.zeros((YS, QB), jnp.int32)
+    key_doc = jnp.zeros((YS, QB), jnp.int32)
+    for i in range(DOCS):
+        end = end + lengths[i]
+        query_doc = query_doc + (query_place >= end).astype(jnp.int32)
+        key_doc = key_doc + (key_place >= end).astype(jnp.int32)
+    query_ref[...] = query_doc
+    key_ref[...] = key_doc
+
+
+def attend_kernel(
+    lengths_ref, query_doc_ref, key_doc_ref, q_ref, kv_ref, out_ref,
+    lengths, sem, k_s, q_s, m_s, l_s, acc_s,
+):
+    lengths_copy = pltpu.make_async_copy(lengths_ref, lengths, sem)
+    lengths_copy.start()
     query_base = lax.axis_index("z") * (YS * QB)
     key_base = lax.axis_index("y") * KB
+    index = lax.broadcasted_iota(jnp.int32, (PAD, QB), 0)
     mine = pl.ds(pl.multiple_of(lax.axis_index("c") * HW, HW), HW)
-    row = lax.broadcasted_iota(jnp.int32, (YS, QB), 0)
-    lane = lax.broadcasted_iota(jnp.int32, (YS, QB), 1)
-    query_doc = doc_of(query_base + row * QB + lane, ends)
-    key_doc = doc_of(key_base + row * (YS * QB) + lane, ends)
-    index = lax.broadcasted_iota(jnp.int32, (PAD, QB), 0)
     for i in range(ZS * CS):
         half = slice((i % CS) * ROWS, (i % CS + 1) * ROWS)
-        same = index[:, half] == key_doc[i // CS : i // CS + 1, half]
+        same = index[:, half] == key_doc_ref[i // CS : i // CS + 1, half]
         part = jnp.where(same, 1.0, 0.0).astype(bf16)
         k_s[i * ROWS : (i + 1) * ROWS, :] = jnp.transpose(
             jnp.concatenate([kv_ref[i, :HW, :], part], axis=0)
@@ -220,21 +232,24 @@
         q_s[i, :HW, :] = jnp.concatenate(
             [q_ref[2 * i, mine, :], q_ref[2 * i + 1, mine, :]], axis=1
         )
-        other = (index != query_doc[i : i + 1]) & (index < DOCS)
+        other = (index != query_doc_ref[i : i + 1, :]) & (index < DOCS)
         q_s[i, HW:, :] = jnp.where(other, NEG, 0.0).astype(bf16)
     m_s[...] = jnp.full(m_s.shape, START, f32)
     l_s[...] = jnp.zeros(l_s.shape, f32)
     acc_s[...] = jnp.zeros(acc_s.shape, f32)
 
-    first = doc_of(query_base, ends)
-    last = doc_of(query_base + (YS * QB - 1), ends)
+    lengths_copy.wait()
+    end = jnp.int32(0)
+    low, high = jnp.int32(0), jnp.int32(1 << 30)
+    for i in range(DOCS):
+        end = end + lengths[i]
+        low = jnp.where(end <= query_base, end, low)
+        high = jnp.minimum(high, jnp.where(end >= query_base + YS * QB, end, 1 << 30))
 
     def key_step(j, _):
         start = key_base + j * (YS * QB)
-        least = doc_of(start, ends)
-        most = doc_of(start + (KB - 1), ends)
-
-        @pl.when((least <= last) & (most >= first))
+
+        @pl.when((start < high) & (start + KB > low))
         def _():
             keys = k_s[pl.ds(pl.multiple_of(j * KB, KB), KB), :]
             values = jnp.concatenate([kv_ref[2 * j, HW:, :], kv_ref[2 * j + 1, HW:, :]], axis=1)
@@ -287,7 +302,7 @@
         out_ref[i, VD:, :] = split_rows(logs, QB)
 
 
-def combine_kernel(in_ref, out_ref):
+def combine_kernel(in_ref, out_hbm, out_s, out_sem):
     logs = [joined_rows(in_ref[i, VD:, :]) for i in range(YS)]
     top = logs[0]
     for v in logs[1:]:
@@ -300,26 +315,26 @@
         mixed = mixed + w * in_ref[i, :VD, :].astype(f32)
     head = (mixed / total).astype(bf16)
     tail = split_rows(top + jnp.log(total), QB)
+    copies = []
     for c in range(CS):
+        out_s[c, :VD, :] = head[:, c * ROWS : (c + 1) * ROWS]
+        out_s[c, VD:, :] = tail[:, c * ROWS : (c + 1) * ROWS]
         for x in range(XS):
-            out_ref[c * XS + x, :VD, :] = head[:, c * ROWS : (c + 1) * ROWS]
-            out_ref[c * XS + x, VD:, :] = tail[:, c * ROWS : (c + 1) * ROWS]
-
-
-def column_kernel(gain_ref, out_ref):
-    gain = gain_ref[...]
-    out_ref[...] = jnp.transpose(jnp.broadcast_to(gain, (ROWS, gain.shape[1])))
-
-
-def output_kernel(x_at, in_ref, first_ref, second_ref, weight_ref, out_ref, log_ref):
+            at = c * XS + x
+            copies.append(pltpu.make_async_copy(out_s.at[c], out_hbm.at[at], out_sem.at[at]))
+            copies[-1].start()
+    for copy in copies:
+        copy.wait()
+
+
+def output_kernel(x_at, in_ref, gain_ref, weight_ref, out_ref, log_ref):
     heads = []
     for x in range(XS):
         for c in range(CS):
             heads.append(in_ref[c * XS + x, :VD, :].astype(f32))
     joined = jnp.concatenate(heads, axis=0)
     square = jnp.sum(joined * joined, axis=0, keepdims=True) * (1.0 / joined.shape[0])
-    gain = jnp.concatenate([first_ref[...], second_ref[...]], axis=0)
-    normed = (joined * lax.rsqrt(square + EPS) * gain).astype(bf16)
+    normed = (joined * lax.rsqrt(square + EPS) * gain_ref[...]).astype(bf16)
     out_ref[...] = lax.dot_general(
         normed, weight_ref[...], (((0,), (0,)), ((), ())), preferred_element_type=f32
     ).astype(bf16)
@@ -339,25 +354,27 @@
     return pl.BlockSpec(memory_space=pltpu.VMEM)
 
 
-def call(kernel, out_shape, scalars, arrays, scratch=()):
+def call(kernel, out_shape, scalars, arrays, scratch=(), spaces=None):
     many = isinstance(out_shape, (tuple, list))
     return pl.pallas_call(
         kernel,
         out_shape=out_shape,
         in_specs=[smem()] * len(scalars) + [vmem()] * len(arrays),
-        out_specs=[vmem() for _ in out_shape] if many else vmem(),
+        out_specs=spaces or ([vmem() for _ in out_shape] if many else vmem()),
         scratch_shapes=list(scratch),
         compiler_params=pltpu.CompilerParams(vmem_limit_bytes=32 * 1024 * 1024),
     )(*scalars, *arrays)
 
 
-def run_attend(doc_lengths, q_all, kv_all):
+def run_attend(doc_lengths, query_docs, key_docs, q_all, kv_all):
     return call(
         attend_kernel,
         jax.ShapeDtypeStruct((YS, MSG, QB), bf16),
-        (doc_lengths,),
-        (q_all, kv_all),
+        (),
+        (doc_lengths, query_docs, key_docs, q_all, kv_all),
         scratch=(
+            pltpu.SMEM((DOCS,), jnp.int32),
+            pltpu.SemaphoreType.DMA(()),
             pltpu.VMEM((ZS * KB, 128), bf16),
             pltpu.VMEM((YS, 128, QB), bf16),
             pltpu.VMEM((YS, 1, QB), f32),
@@ -388,7 +405,7 @@
         start_kernel,
         out_shape=jax.ShapeDtypeStruct((XS, ROPE_AT + 8, 128), bf16),
         in_specs=[hbm()] * 6,
-        out_specs=vmem(),
+        out_specs=hbm(),
         scratch_shapes=[
             pltpu.VMEM(tokens.shape, bf16),
             pltpu.VMEM(query_down.shape, bf16),
@@ -396,9 +413,11 @@
             pltpu.VMEM(rope_down.shape[::-1], bf16),
             pltpu.VMEM((1, *query_latent_gain.shape), f32),
             pltpu.VMEM((1, *latent_gain.shape), f32),
+            pltpu.VMEM((ROPE_AT + 8, 128), bf16),
             pltpu.SemaphoreType.DMA((4,)),
             pltpu.SemaphoreType.DMA((STEPS,)),
             pltpu.SemaphoreType.DMA((STEPS,)),
+            pltpu.SemaphoreType.DMA((XS,)),
         ],
         compiler_params=pltpu.CompilerParams(vmem_limit_bytes=63 * 1024 * 1024),
         name="start",
@@ -418,6 +437,8 @@
     angles = places.astype(f32)[None, :] * inverse[:, None]
     cosine, sine = jnp.cos(angles), jnp.sin(angles)
 
+    docs = jax.ShapeDtypeStruct((YS, QB), jnp.int32)
+    query_docs, key_docs = call(table_kernel, (docs, docs), (doc_lengths,), ())
     kv_out, q_out = call(
         proj_kernel,
         (
@@ -435,17 +456,22 @@
             cosine,
             sine,
         ),
+        scratch=(pltpu.VMEM((CS, KV, ROWS), bf16), pltpu.SemaphoreType.DMA((ZS * CS,))),
+        spaces=[hbm(), vmem()],
     )
     kv_all = lax.all_to_all(kv_out, ("z", "c"), split_axis=0, concat_axis=0, tiled=True)
     q_all = lax.all_gather(q_out, ("y", "c"), axis=0)
 
-    parts = run_attend(doc_lengths, q_all, kv_all)
+    parts = run_attend(doc_lengths, query_docs, key_docs, q_all, kv_all)
     parts = lax.all_to_all(parts, "y", split_axis=0, concat_axis=0, tiled=True)
-    half = output_gain.shape[0] // 2
-    column = jax.ShapeDtypeStruct((half, ROWS), f32)
-    first = call(column_kernel, column, (), (output_gain[:half].reshape(1, -1),))
-    second = call(column_kernel, column, (), (output_gain[half:].reshape(1, -1),))
-    heads = call(combine_kernel, jax.ShapeDtypeStruct((CS * XS, MSG, ROWS), bf16), (), (parts,))
+    heads = call(
+        combine_kernel,
+        jax.ShapeDtypeStruct((CS * XS, MSG, ROWS), bf16),
+        (),
+        (parts,),
+        scratch=(pltpu.VMEM((CS, MSG, ROWS), bf16), pltpu.SemaphoreType.DMA((CS * XS,))),
+        spaces=hbm(),
+    )
     heads = lax.all_to_all(heads, ("c", "x"), split_axis=0, concat_axis=0, tiled=True)
     layer_output, log_totals = call(
         output_kernel,
@@ -454,7 +480,7 @@
             jax.ShapeDtypeStruct((CS, ROWS), f32),
         ),
         (x_at.astype(jnp.int32).reshape(1),),
-        (heads, first, second, output_weight),
+        (heads, output_gain[:, None], output_weight),
     )
     return (layer_output, log_totals)
 

time: 84.4 us -> 82.8 us (0.981)
  blocking collectives: 19.8 us -> 37.9 us
  waiting for transfers between devices: 21.8 us -> 9.28 us
  starting transfers between devices: 27.4 us -> 20.6 us
    all_to_all x0 -> x1, blocking collectives: none -> 18.1 us  [per_device(): parts = lax.all_to_all(parts, 'y', split_axis=0, concat_axis=0, tiled=True)]
    all_to_all x1 -> x0, waiting for transfers between devices: 12 us -> none  [per_device(): parts = lax.all_to_all(parts, 'y', split_axis=0, concat_axis=0, tiled=True)]
    all_to_all x1 -> x0, starting transfers between devices: 6.83 us -> none  [per_device(): parts = lax.all_to_all(parts, 'y', split_axis=0, concat_axis=0, tiled=True)]
    pallas_call x6 -> x5, Pallas kernels: 10.4 us -> 9.72 us  [call(): pl.pallas_call(kernel, out_shape=out_shape, in_specs=[smem()] * len(scala...]
  transfers between devices with their start and end apart: 4 -> 3, of which waited for: 4 -> 2; matrix products, arithmetic and copies ran while one was open for 0% -> 1% of each run, Pallas kernels for 0% -> 1%
where the time goes in v1:
time: 82.8 us; the launch traced here: 82.4 us
  blocking collectives  37.9 us (46%)
  starting transfers between devices  20.6 us (25%)
  Pallas kernels  13.2 us (16%)
  waiting for transfers between devices  9.28 us (11%)
    all_gather x1, blocking collectives, per_device(): q_all = lax.all_gather(q_out, ('y', 'c'), axis=0)  19.8 us
    all_to_all x1, blocking collectives, per_device(): parts = lax.all_to_all(parts, 'y', split_axis=0, concat_axis=0, tiled=True)  18.1 us
    all_to_all x1, starting transfers between devices, per_device(): lax.all_to_all(kv_out, ('z', 'c'), split_axis=0, concat_axis=0, tiled=True)  12.4 us
    pallas_call x5, Pallas kernels, call(): pl.pallas_call(kernel, out_shape=out_shape, in_specs=[smem()] * len(scala...  9.72 us
    all_to_all x1, waiting for transfers between devices, per_device(): every = lax.all_to_all(packed, 'x', split_axis=0, concat_axis=0, tiled=True)  4.85 us
    all_to_all x1, starting transfers between devices, per_device(): every = lax.all_to_all(packed, 'x', split_axis=0, concat_axis=0, tiled=True)  4.84 us
    all_to_all x1, waiting for transfers between devices, per_device(): lax.all_to_all(heads, ('c', 'x'), split_axis=0, concat_axis=0, tiled=True)  4.43 us
    pallas_call x1, Pallas kernels, per_device(): pl.pallas_call(start_kernel, out_shape=jax.ShapeDtypeStruct((XS, ROPE_AT...  3.47 us
  transfers between devices with their start and end apart: 3, of which 2 were waited for; matrix products, arithmetic and copies ran while one was open for 1% of the time, Pallas kernels for 1%

profile of v1, /device:TPU:1, one launch (start us, length us, event | category | flops | bytes accessed | tf_op | source)
XLA Modules:
  0.0 82.4 jit_solution(6100520392531571096)
XLA Ops:
  0.6 0.0 copy-start.6
  0.6 0.0 copy-start.7
  0.7 0.0 copy-start.3
  0.7 0.0 copy-start.2
  0.7 0.0 copy-start.1
  0.7 3.5 %start.1 = bf16[4,200,128]{2,1,0:T(8,128)(2,1)} custom-call(bf16[32,2048]{1,0:T(8,128)(2,1)} %tok_hbm.1, bf16[2048,512]{1,0:T(8,128)(2,1)} %query_hbm.1, bf16[2048,256]{1,0:T(8,128)(2,1)} %latent_hbm.1, bf16[32,2048]{1,0:T(8,128)(2,1)} %bitcast.11, f32[1,512]{1,0:T(1,128)} %bitcast.12, f32[1,256]{1,0:T(1,128)} %bitcast.14), custom_call_target="tpu_custom_call" | custom-call | tf_op jit(solution)/shard_map/start/pallas_call | solution.py:404
  4.2 0.0 copy-start.4
  4.2 4.8 %all-to-all-start = ((bf16[4,200,128]{2,1,0:T(8,128)(2,1)}), bf16[4,200,128]{2,1,0:T(8,128)(2,1)S(1)}, u32[]{:S(2)}, u32[]{:S(2)}) async-start(bf16[4,200,128]{2,1,0:T(8,128)(2,1)} %start.1), calls=%async_computation | async-start | bytes 409600 | tf_op jit(solution)/shard_map/all_to_all | solution.py:432
  9.0 0.0 copy-done.6
  9.1 0.1 copy.19.query_gain_ref
  9.2 0.0 copy-done.7
  9.2 0.1 copy.18.key_gain_ref
  9.3 0.1 multiply_sine_fusion
  9.4 4.8 %all-to-all-done.in_ref = bf16[4,200,128]{2,1,0:T(8,128)(2,1)S(1)} async-done(((bf16[4,200,128]{2,1,0:T(8,128)(2,1)}), bf16[4,200,128]{2,1,0:T(8,128)(2,1)S(1)}, u32[]{:S(2)}, u32[]{:S(2)}) %all-to-all-start) | async-done | bytes 204832 | tf_op jit(solution)/shard_map/all_to_all | solution.py:432
  14.2 0.0 copy-done.3
  14.2 0.0 copy-done.2
  14.2 0.0 copy-done.1
  14.2 1.2 %shard_map.150 = (bf16[16,160,128]{2,1,0:T(8,128)(2,1)}, bf16[192,128]{1,0:T(8,128)(2,1)S(1)}) custom-call(bf16[4,200,128]{2,1,0:T(8,128)(2,1)S(1)} %all-to-all-done.in_ref, bf16[256,128]{1,0:T(8,128)(2,1)S(1)} %copy-done.2, bf16[256,128]{1,0:T(8,128)(2,1)S(1)} %copy-done.3, bf16[192,512]{1,0:T(8,128)(2,1)S(1)} %bitcast.10, f32[96,1]{1,0:T(8,128)S(1)} %copy.18.key_gain_ref, ...), custom_call_target="tpu_custom_call" | custom-call | tf_op jit(solution)/shard_map/pallas_call | solution.py:359
  15.5 12.4 %all-to-all-start.1 = ((bf16[16,160,128]{2,1,0:T(8,128)(2,1)}), bf16[16,160,128]{2,1,0:T(8,128)(2,1)S(1)}, u32[]{:S(2)}, u32[]{:S(2)}) async-start(bf16[16,160,128]{2,1,0:T(8,128)(2,1)} %get-tuple-element.9), calls=%async_computation.1 | async-start | bytes 1310720 | tf_op jit(solution)/shard_map/all_to_all | solution.py:462
  27.9 0.0 copy-done.4
  27.9 0.0 copy-start.5
  28.0 0.6 shard_map.149
  28.5 0.0 copy-start
  28.6 19.8 %all-gather = bf16[3072,128]{1,0:T(8,128)(2,1)S(1)} all-gather(bf16[192,128]{1,0:T(8,128)(2,1)S(1)} %get-tuple-element.8), channel_id=2, replica_groups=mesh['z'=8,'y'=8,'c'=2,'x'=4] {'y','c'}, dimensions={0}, use_global_device_ids=true | all-gather | bytes 835584 | tf_op jit(solution)/shard_map/all_gather | solution.py:463
  48.4 0.0 all-to-all-done.1.kv_ref
  48.4 6.0 %shard_map.151 = bf16[8,72,256]{2,1,0:T(8,128)(2,1)S(1)} custom-call(s32[16]{0:T(128)S(1)} %copy-done.4, s32[8,256]{1,0:T(8,128)S(1)} %get-tuple-element.6.query_doc_ref, s32[8,256]{1,0:T(8,128)S(1)} %get-tuple-element.7.key_doc_ref, bf16[16,192,128]{2,1,0:T(8,128)(2,1)S(1)} %bitcast.9, bf16[16,160,128]{2,1,0:T(8,128)(2,1)S(1)} %all-to-all-done.1.kv_ref), custom_call_target="tpu_custom_call" | custom-call | tf_op jit(solution)/shard_map/pallas_call | solution.py:359
  54.4 18.1 %all_to_all.20.in_ref = bf16[8,72,256]{2,1,0:T(8,128)(2,1)S(1)} all-to-all(bf16[8,72,256]{2,1,0:T(8,128)(2,1)S(1)} %shard_map.151), channel_id=1, replica_groups=mesh['z'=8,'y'=8,'c'=2,'x'=4] {'y'}, dimensions={0} | all-to-all | bytes 589824 | tf_op jit(solution)/shard_map/all_to_all | solution.py:466
  72.6 0.8 %shard_map.152 = bf16[8,72,128]{2,1,0:T(8,128)(2,1)} custom-call(bf16[8,72,256]{2,1,0:T(8,128)(2,1)S(1)} %all_to_all.20.in_ref), custom_call_target="tpu_custom_call" | custom-call | tf_op jit(solution)/shard_map/pallas_call | solution.py:359
  73.4 3.3 %all-to-all-start.3 = ((bf16[8,72,128]{2,1,0:T(8,128)(2,1)}), bf16[8,72,128]{2,1,0:T(8,128)(2,1)S(1)}, u32[]{:S(2)}, u32[]{:S(2)}) async-start(bf16[8,72,128]{2,1,0:T(8,128)(2,1)} %shard_map.152), calls=%async_computation.3 | async-start | bytes 294912 | tf_op jit(solution)/shard_map/all_to_all | solution.py:475
  76.7 0.0 copy-done.5
  76.7 0.1 copy.20.gain_ref
  76.9 4.4 %all-to-all-done.3.in_ref = bf16[8,72,128]{2,1,0:T(8,128)(2,1)S(1)} async-done(((bf16[8,72,128]{2,1,0:T(8,128)(2,1)}), bf16[8,72,128]{2,1,0:T(8,128)(2,1)S(1)}, u32[]{:S(2)}, u32[]{:S(2)}) %all-to-all-start.3) | async-done | bytes 147488 | tf_op jit(solution)/shard_map/all_to_all | solution.py:475
  81.3 0.0 copy-done
  81.3 1.0 %shard_map.153 = (bf16[128,512]{1,0:T(8,128)(2,1)}, f32[2,128]{1,0:T(2,128)}) custom-call(s32[1]{0:T(128)} %bitcast.x_at, bf16[8,72,128]{2,1,0:T(8,128)(2,1)S(1)} %all-to-all-done.3.in_ref, f32[512,1]{1,0:T(8,128)S(1)} %copy.20.gain_ref, bf16[512,512]{1,0:T(8,128)(2,1)S(1)} %copy-done), custom_call_target="tpu_custom_call" | custom-call | tf_op jit(solution)/shard_map/pallas_call | solution.py:359
  (2 shorter events, 0.0 us)
Async XLA Ops:
  0.6 8.4 %copy-start.6 = (f32[96]{0:T(128)S(1)}, f32[96]{0:T(128)}, u32[]{:S(2)}) copy-start(f32[96]{0:T(128)} %param.24) | copy-start | bytes 1156
  0.6 8.5 %copy-start.7 = (f32[96]{0:T(128)S(1)}, f32[96]{0:T(128)}, u32[]{:S(2)}) copy-start(f32[96]{0:T(128)} %param.25) | copy-start | bytes 1156
  0.7 13.6 %copy-start.3 = (bf16[256,128]{1,0:T(8,128)(2,1)S(1)}, bf16[256,128]{1,0:T(8,128)(2,1)}, u32[]{:S(2)}) copy-start(bf16[256,128]{1,0:T(8,128)(2,1)} %value_up_ref.1) | copy-start | bytes 196612
  0.7 13.6 %copy-start.2 = (bf16[256,128]{1,0:T(8,128)(2,1)S(1)}, bf16[256,128]{1,0:T(8,128)(2,1)}, u32[]{:S(2)}) copy-start(bf16[256,128]{1,0:T(8,128)(2,1)} %key_up_ref.1) | copy-start | bytes 196612
  0.7 13.6 %copy-start.1 = (bf16[512,192]{0,1:T(8,128)(2,1)S(1)}, bf16[512,192]{0,1:T(8,128)(2,1)}, u32[]{:S(2)}) copy-start(bf16[512,192]{0,1:T(8,128)(2,1)} %param.21) | copy-start | bytes 589828
  4.2 23.8 %copy-start.4 = (s32[16]{0:T(128)S(1)}, s32[16]{0:T(128)}, u32[]{:S(2)}) copy-start(s32[16]{0:T(128)} %lengths_ref.1) | copy-start | bytes 196
  4.2 10.1 %all-to-all-start = ((bf16[4,200,128]{2,1,0:T(8,128)(2,1)}), bf16[4,200,128]{2,1,0:T(8,128)(2,1)S(1)}, u32[]{:S(2)}, u32[]{:S(2)}) async-start(bf16[4,200,128]{2,1,0:T(8,128)(2,1)} %start.1), calls=%async_computation | async-start | bytes 409600 | tf_op jit(solution)/shard_map/all_to_all | solution.py:432
  15.5 32.9 %all-to-all-start.1 = ((bf16[16,160,128]{2,1,0:T(8,128)(2,1)}), bf16[16,160,128]{2,1,0:T(8,128)(2,1)S(1)}, u32[]{:S(2)}, u32[]{:S(2)}) async-start(bf16[16,160,128]{2,1,0:T(8,128)(2,1)} %get-tuple-element.9), calls=%async_computation.1 | async-start | bytes 1310720 | tf_op jit(solution)/shard_map/all_to_all | solution.py:462
  27.9 48.8 %copy-start.5 = (f32[512]{0:T(512)S(1)}, f32[512]{0:T(512)}, u32[]{:S(2)}) copy-start(f32[512]{0:T(512)} %param.26) | copy-start | bytes 6148
  28.5 52.8 %copy-start = (bf16[512,512]{1,0:T(8,128)(2,1)S(1)}, bf16[512,512]{1,0:T(8,128)(2,1)}, u32[]{:S(2)}) copy-start(bf16[512,512]{1,0:T(8,128)(2,1)} %weight_ref.1) | copy-start | bytes 1572868
  73.4 7.9 %all-to-all-start.3 = ((bf16[8,72,128]{2,1,0:T(8,128)(2,1)}), bf16[8,72,128]{2,1,0:T(8,128)(2,1)S(1)}, u32[]{:S(2)}, u32[]{:S(2)}) async-start(bf16[8,72,128]{2,1,0:T(8,128)(2,1)} %shard_map.152), calls=%async_computation.3 | async-start | bytes 294912 | tf_op jit(solution)/shard_map/all_to_all | solution.py:475

commit v2 on v0

--- a/solution.py
+++ b/solution.py
@@ -185,33 +185,35 @@
 PAD = 128 - HW
 
 
-def ends_of(lengths):
-    ends = [lengths[0]]
-    for i in range(1, DOCS):
-        ends.append(ends[-1] + lengths[i])
-    return ends
-
-
-def doc_of(place, ends):
-    doc = (place >= ends[0]).astype(jnp.int32)
-    for end in ends[1:]:
-        doc = doc + (place >= end).astype(jnp.int32)
-    return doc
-
-
-def attend_kernel(lengths, q_ref, kv_ref, out_ref, k_s, q_s, m_s, l_s, acc_s):
-    ends = ends_of(lengths)
+def table_kernel(lengths, query_ref, key_ref):
+    row = lax.broadcasted_iota(jnp.int32, (YS, QB), 0)
+    lane = lax.broadcasted_iota(jnp.int32, (YS, QB), 1)
+    query_place = lax.axis_index("z") * (YS * QB) + row * QB + lane
+    key_place = lax.axis_index("y") * KB + row * (YS * QB) + lane
+    end = jnp.int32(0)
+    query_doc = jnp.zeros((YS, QB), jnp.int32)
+    key_doc = jnp.zeros((YS, QB), jnp.int32)
+    for i in range(DOCS):
+        end = end + lengths[i]
+        query_doc = query_doc + (query_place >= end).astype(jnp.int32)
+        key_doc = key_doc + (key_place >= end).astype(jnp.int32)
+    query_ref[...] = query_doc
+    key_ref[...] = key_doc
+
+
+def attend_kernel(
+    lengths_ref, query_doc_ref, key_doc_ref, q_ref, kv_ref, out_ref,
+    lengths, sem, k_s, q_s, m_s, l_s, acc_s,
+):
+    lengths_copy = pltpu.make_async_copy(lengths_ref, lengths, sem)
+    lengths_copy.start()
     query_base = lax.axis_index("z") * (YS * QB)
     key_base = lax.axis_index("y") * KB
+    index = lax.broadcasted_iota(jnp.int32, (PAD, QB), 0)
     mine = pl.ds(pl.multiple_of(lax.axis_index("c") * HW, HW), HW)
-    row = lax.broadcasted_iota(jnp.int32, (YS, QB), 0)
-    lane = lax.broadcasted_iota(jnp.int32, (YS, QB), 1)
-    query_doc = doc_of(query_base + row * QB + lane, ends)
-    key_doc = doc_of(key_base + row * (YS * QB) + lane, ends)
-    index = lax.broadcasted_iota(jnp.int32, (PAD, QB), 0)
     for i in range(ZS * CS):
         half = slice((i % CS) * ROWS, (i % CS + 1) * ROWS)
-        same = index[:, half] == key_doc[i // CS : i // CS + 1, half]
+        same = index[:, half] == key_doc_ref[i // CS : i // CS + 1, half]
         part = jnp.where(same, 1.0, 0.0).astype(bf16)
         k_s[i * ROWS : (i + 1) * ROWS, :] = jnp.transpose(
             jnp.concatenate([kv_ref[i, :HW, :], part], axis=0)
@@ -220,21 +222,24 @@
         q_s[i, :HW, :] = jnp.concatenate(
             [q_ref[2 * i, mine, :], q_ref[2 * i + 1, mine, :]], axis=1
         )
-        other = (index != query_doc[i : i + 1]) & (index < DOCS)
+        other = (index != query_doc_ref[i : i + 1, :]) & (index < DOCS)
         q_s[i, HW:, :] = jnp.where(other, NEG, 0.0).astype(bf16)
     m_s[...] = jnp.full(m_s.shape, START, f32)
     l_s[...] = jnp.zeros(l_s.shape, f32)
     acc_s[...] = jnp.zeros(acc_s.shape, f32)
 
-    first = doc_of(query_base, ends)
-    last = doc_of(query_base + (YS * QB - 1), ends)
+    lengths_copy.wait()
+    end = jnp.int32(0)
+    low, high = jnp.int32(0), jnp.int32(1 << 30)
+    for i in range(DOCS):
+        end = end + lengths[i]
+        low = jnp.where(end <= query_base, end, low)
+        high = jnp.minimum(high, jnp.where(end >= query_base + YS * QB, end, 1 << 30))
 
     def key_step(j, _):
         start = key_base + j * (YS * QB)
-        least = doc_of(start, ends)
-        most = doc_of(start + (KB - 1), ends)
-
-        @pl.when((least <= last) & (most >= first))
+
+        @pl.when((start < high) & (start + KB > low))
         def _():
             keys = k_s[pl.ds(pl.multiple_of(j * KB, KB), KB), :]
             values = jnp.concatenate([kv_ref[2 * j, HW:, :], kv_ref[2 * j + 1, HW:, :]], axis=1)
@@ -306,20 +311,14 @@
             out_ref[c * XS + x, VD:, :] = tail[:, c * ROWS : (c + 1) * ROWS]
 
 
-def column_kernel(gain_ref, out_ref):
-    gain = gain_ref[...]
-    out_ref[...] = jnp.transpose(jnp.broadcast_to(gain, (ROWS, gain.shape[1])))
-
-
-def output_kernel(x_at, in_ref, first_ref, second_ref, weight_ref, out_ref, log_ref):
+def output_kernel(x_at, in_ref, gain_ref, weight_ref, out_ref, log_ref):
     heads = []
     for x in range(XS):
         for c in range(CS):
             heads.append(in_ref[c * XS + x, :VD, :].astype(f32))
     joined = jnp.concatenate(heads, axis=0)
     square = jnp.sum(joined * joined, axis=0, keepdims=True) * (1.0 / joined.shape[0])
-    gain = jnp.concatenate([first_ref[...], second_ref[...]], axis=0)
-    normed = (joined * lax.rsqrt(square + EPS) * gain).astype(bf16)
+    normed = (joined * lax.rsqrt(square + EPS) * gain_ref[...]).astype(bf16)
     out_ref[...] = lax.dot_general(
         normed, weight_ref[...], (((0,), (0,)), ((), ())), preferred_element_type=f32
     ).astype(bf16)
@@ -351,13 +350,15 @@
     )(*scalars, *arrays)
 
 
-def run_attend(doc_lengths, q_all, kv_all):
+def run_attend(doc_lengths, query_docs, key_docs, q_all, kv_all):
     return call(
         attend_kernel,
         jax.ShapeDtypeStruct((YS, MSG, QB), bf16),
-        (doc_lengths,),
-        (q_all, kv_all),
+        (),
+        (doc_lengths, query_docs, key_docs, q_all, kv_all),
         scratch=(
+            pltpu.SMEM((DOCS,), jnp.int32),
+            pltpu.SemaphoreType.DMA(()),
             pltpu.VMEM((ZS * KB, 128), bf16),
             pltpu.VMEM((YS, 128, QB), bf16),
             pltpu.VMEM((YS, 1, QB), f32),
@@ -418,6 +419,8 @@
     angles = places.astype(f32)[None, :] * inverse[:, None]
     cosine, sine = jnp.cos(angles), jnp.sin(angles)
 
+    docs = jax.ShapeDtypeStruct((YS, QB), jnp.int32)
+    query_docs, key_docs = call(table_kernel, (docs, docs), (doc_lengths,), ())
     kv_out, q_out = call(
         proj_kernel,
         (
@@ -439,12 +442,8 @@
     kv_all = lax.all_to_all(kv_out, ("z", "c"), split_axis=0, concat_axis=0, tiled=True)
     q_all = lax.all_gather(q_out, ("y", "c"), axis=0)
 
-    parts = run_attend(doc_lengths, q_all, kv_all)
+    parts = run_attend(doc_lengths, query_docs, key_docs, q_all, kv_all)
     parts = lax.all_to_all(parts, "y", split_axis=0, concat_axis=0, tiled=True)
-    half = output_gain.shape[0] // 2
-    column = jax.ShapeDtypeStruct((half, ROWS), f32)
-    first = call(column_kernel, column, (), (output_gain[:half].reshape(1, -1),))
-    second = call(column_kernel, column, (), (output_gain[half:].reshape(1, -1),))
     heads = call(combine_kernel, jax.ShapeDtypeStruct((CS * XS, MSG, ROWS), bf16), (), (parts,))
     heads = lax.all_to_all(heads, ("c", "x"), split_axis=0, concat_axis=0, tiled=True)
     layer_output, log_totals = call(
@@ -454,7 +453,7 @@
             jax.ShapeDtypeStruct((CS, ROWS), f32),
         ),
         (x_at.astype(jnp.int32).reshape(1),),
-        (heads, first, second, output_weight),
+        (heads, output_gain[:, None], output_weight),
     )
     return (layer_output, log_totals)
 

time: 84.4 us -> 82.4 us (0.976)
  blocking collectives: 19.8 us -> 37.9 us
  waiting for transfers between devices: 21.8 us -> 9.27 us
  starting transfers between devices: 27.4 us -> 20.6 us
    all_to_all x0 -> x1, blocking collectives: none -> 18.1 us  [per_device(): parts = lax.all_to_all(parts, 'y', split_axis=0, concat_axis=0, tiled=True)]
    all_to_all x1 -> x0, waiting for transfers between devices: 12 us -> none  [per_device(): parts = lax.all_to_all(parts, 'y', split_axis=0, concat_axis=0, tiled=True)]
    all_to_all x1 -> x0, starting transfers between devices: 6.83 us -> none  [per_device(): parts = lax.all_to_all(parts, 'y', split_axis=0, concat_axis=0, tiled=True)]
    pallas_call x6 -> x5, Pallas kernels: 10.4 us -> 9.55 us  [call(): pl.pallas_call(kernel, out_shape=out_shape, in_specs=[smem()] * len(scala...]
  transfers between devices with their start and end apart: 4 -> 3, of which waited for: 4 -> 2; matrix products, arithmetic and copies ran while one was open for 0% -> 1% of each run, Pallas kernels for 0% -> 1%
where the time goes in v2:
time: 82.4 us; the launch traced here: 82 us
  blocking collectives  37.9 us (46%)
  starting transfers between devices  20.6 us (25%)
  Pallas kernels  12.9 us (16%)
  waiting for transfers between devices  9.27 us (11%)
    all_gather x1, blocking collectives, per_device(): q_all = lax.all_gather(q_out, ('y', 'c'), axis=0)  19.8 us
    all_to_all x1, blocking collectives, per_device(): parts = lax.all_to_all(parts, 'y', split_axis=0, concat_axis=0, tiled=True)  18.1 us
    all_to_all x1, starting transfers between devices, per_device(): lax.all_to_all(kv_out, ('z', 'c'), split_axis=0, concat_axis=0, tiled=True)  12.4 us
    pallas_call x5, Pallas kernels, call(): pl.pallas_call(kernel, out_shape=out_shape, in_specs=[smem()] * len(scala...  9.55 us
    all_to_all x1, waiting for transfers between devices, per_device(): every = lax.all_to_all(packed, 'x', split_axis=0, concat_axis=0, tiled=True)  4.85 us
    all_to_all x1, starting transfers between devices, per_device(): every = lax.all_to_all(packed, 'x', split_axis=0, concat_axis=0, tiled=True)  4.84 us
    all_to_all x1, waiting for transfers between devices, per_device(): lax.all_to_all(heads, ('c', 'x'), split_axis=0, concat_axis=0, tiled=True)  4.42 us
    all_to_all x1, starting transfers between devices, per_device(): lax.all_to_all(heads, ('c', 'x'), split_axis=0, concat_axis=0, tiled=True)  3.33 us
  transfers between devices with their start and end apart: 3, of which 2 were waited for; matrix products, arithmetic and copies ran while one was open for 1% of the time, Pallas kernels for 1%

profile of v2, /device:TPU:1, one launch (start us, length us, event | category | flops | bytes accessed | tf_op | source)
XLA Modules:
  0.0 82.0 jit_solution(6980744478585582322)
XLA Ops:
  0.6 0.0 copy-start.6
  0.6 0.0 copy-start.7
  0.7 0.0 copy-start.3
  0.7 0.0 copy-start.2
  0.7 0.0 copy-start.1
  0.7 3.3 %start.1 = bf16[4,200,128]{2,1,0:T(8,128)(2,1)} custom-call(bf16[32,2048]{1,0:T(8,128)(2,1)} %tok_hbm.1, bf16[2048,512]{1,0:T(8,128)(2,1)} %query_hbm.1, bf16[2048,256]{1,0:T(8,128)(2,1)} %latent_hbm.1, bf16[32,2048]{1,0:T(8,128)(2,1)} %bitcast.11, f32[1,512]{1,0:T(1,128)} %bitcast.12, f32[1,256]{1,0:T(1,128)} %bitcast.14), custom_call_target="tpu_custom_call" | custom-call | tf_op jit(solution)/shard_map/start/pallas_call | solution.py:388
  4.0 0.0 copy-start.4
  4.0 4.8 %all-to-all-start = ((bf16[4,200,128]{2,1,0:T(8,128)(2,1)}), bf16[4,200,128]{2,1,0:T(8,128)(2,1)S(1)}, u32[]{:S(2)}, u32[]{:S(2)}) async-start(bf16[4,200,128]{2,1,0:T(8,128)(2,1)} %start.1), calls=%async_computation | async-start | bytes 409600 | tf_op jit(solution)/shard_map/all_to_all | solution.py:414
  8.9 0.0 copy-done.6
  8.9 0.1 copy.19.query_gain_ref
  9.0 0.0 copy-done.7
  9.0 0.1 copy.18.key_gain_ref
  9.1 0.1 multiply_sine_fusion
  9.2 4.8 %all-to-all-done.in_ref = bf16[4,200,128]{2,1,0:T(8,128)(2,1)S(1)} async-done(((bf16[4,200,128]{2,1,0:T(8,128)(2,1)}), bf16[4,200,128]{2,1,0:T(8,128)(2,1)S(1)}, u32[]{:S(2)}, u32[]{:S(2)}) %all-to-all-start) | async-done | bytes 204832 | tf_op jit(solution)/shard_map/all_to_all | solution.py:414
  14.1 0.0 copy-done.3
  14.1 0.0 copy-done.2
  14.1 0.0 copy-done.1
  14.1 1.1 %shard_map.150 = (bf16[16,160,128]{2,1,0:T(8,128)(2,1)}, bf16[192,128]{1,0:T(8,128)(2,1)S(1)}) custom-call(bf16[4,200,128]{2,1,0:T(8,128)(2,1)S(1)} %all-to-all-done.in_ref, bf16[256,128]{1,0:T(8,128)(2,1)S(1)} %copy-done.2, bf16[256,128]{1,0:T(8,128)(2,1)S(1)} %copy-done.3, bf16[192,512]{1,0:T(8,128)(2,1)S(1)} %bitcast.10, f32[96,1]{1,0:T(8,128)S(1)} %copy.18.key_gain_ref, ...), custom_call_target="tpu_custom_call" | custom-call | tf_op jit(solution)/shard_map/pallas_call | solution.py:343
  15.2 12.4 %all-to-all-start.1 = ((bf16[16,160,128]{2,1,0:T(8,128)(2,1)}), bf16[16,160,128]{2,1,0:T(8,128)(2,1)S(1)}, u32[]{:S(2)}, u32[]{:S(2)}) async-start(bf16[16,160,128]{2,1,0:T(8,128)(2,1)} %get-tuple-element.9), calls=%async_computation.1 | async-start | bytes 1310720 | tf_op jit(solution)/shard_map/all_to_all | solution.py:442
  27.6 0.0 copy-done.4
  27.7 0.0 copy-start.5
  27.7 0.6 shard_map.149
  28.3 0.0 copy-start
  28.3 19.8 %all-gather = bf16[3072,128]{1,0:T(8,128)(2,1)S(1)} all-gather(bf16[192,128]{1,0:T(8,128)(2,1)S(1)} %get-tuple-element.8), channel_id=2, replica_groups=mesh['z'=8,'y'=8,'c'=2,'x'=4] {'y','c'}, dimensions={0}, use_global_device_ids=true | all-gather | bytes 835584 | tf_op jit(solution)/shard_map/all_gather | solution.py:443
  48.1 0.0 all-to-all-done.1.kv_ref
  48.1 6.0 %shard_map.151 = bf16[8,72,256]{2,1,0:T(8,128)(2,1)S(1)} custom-call(s32[16]{0:T(128)S(1)} %copy-done.4, s32[8,256]{1,0:T(8,128)S(1)} %get-tuple-element.6.query_doc_ref, s32[8,256]{1,0:T(8,128)S(1)} %get-tuple-element.7.key_doc_ref, bf16[16,192,128]{2,1,0:T(8,128)(2,1)S(1)} %bitcast.9, bf16[16,160,128]{2,1,0:T(8,128)(2,1)S(1)} %all-to-all-done.1.kv_ref), custom_call_target="tpu_custom_call" | custom-call | tf_op jit(solution)/shard_map/pallas_call | solution.py:343
  54.1 18.1 %all_to_all.20.in_ref = bf16[8,72,256]{2,1,0:T(8,128)(2,1)S(1)} all-to-all(bf16[8,72,256]{2,1,0:T(8,128)(2,1)S(1)} %shard_map.151), channel_id=1, replica_groups=mesh['z'=8,'y'=8,'c'=2,'x'=4] {'y'}, dimensions={0} | all-to-all | bytes 589824 | tf_op jit(solution)/shard_map/all_to_all | solution.py:446
  72.3 0.8 shard_map.152
  73.0 3.3 %all-to-all-start.3 = ((bf16[8,72,128]{2,1,0:T(8,128)(2,1)}), bf16[8,72,128]{2,1,0:T(8,128)(2,1)S(1)}, u32[]{:S(2)}, u32[]{:S(2)}) async-start(bf16[8,72,128]{2,1,0:T(8,128)(2,1)} %shard_map.152), calls=%async_computation.3 | async-start | bytes 294912 | tf_op jit(solution)/shard_map/all_to_all | solution.py:448
  76.4 0.0 copy-done.5
  76.4 0.1 copy.20.gain_ref
  76.5 4.4 %all-to-all-done.3.in_ref = bf16[8,72,128]{2,1,0:T(8,128)(2,1)S(1)} async-done(((bf16[8,72,128]{2,1,0:T(8,128)(2,1)}), bf16[8,72,128]{2,1,0:T(8,128)(2,1)S(1)}, u32[]{:S(2)}, u32[]{:S(2)}) %all-to-all-start.3) | async-done | bytes 147488 | tf_op jit(solution)/shard_map/all_to_all | solution.py:448
  80.9 0.0 copy-done
  80.9 1.0 %shard_map.153 = (bf16[128,512]{1,0:T(8,128)(2,1)}, f32[2,128]{1,0:T(2,128)}) custom-call(s32[1]{0:T(128)} %bitcast.x_at, bf16[8,72,128]{2,1,0:T(8,128)(2,1)S(1)} %all-to-all-done.3.in_ref, f32[512,1]{1,0:T(8,128)S(1)} %copy.20.gain_ref, bf16[512,512]{1,0:T(8,128)(2,1)S(1)} %copy-done), custom_call_target="tpu_custom_call" | custom-call | tf_op jit(solution)/shard_map/pallas_call | solution.py:343
  (2 shorter events, 0.0 us)
Async XLA Ops:
  0.6 8.3 %copy-start.6 = (f32[96]{0:T(128)S(1)}, f32[96]{0:T(128)}, u32[]{:S(2)}) copy-start(f32[96]{0:T(128)} %param.24) | copy-start | bytes 1156
  0.6 8.4 %copy-start.7 = (f32[96]{0:T(128)S(1)}, f32[96]{0:T(128)}, u32[]{:S(2)}) copy-start(f32[96]{0:T(128)} %param.25) | copy-start | bytes 1156
  0.7 13.4 %copy-start.3 = (bf16[256,128]{1,0:T(8,128)(2,1)S(1)}, bf16[256,128]{1,0:T(8,128)(2,1)}, u32[]{:S(2)}) copy-start(bf16[256,128]{1,0:T(8,128)(2,1)} %value_up_ref.1) | copy-start | bytes 196612
  0.7 13.4 %copy-start.2 = (bf16[256,128]{1,0:T(8,128)(2,1)S(1)}, bf16[256,128]{1,0:T(8,128)(2,1)}, u32[]{:S(2)}) copy-start(bf16[256,128]{1,0:T(8,128)(2,1)} %key_up_ref.1) | copy-start | bytes 196612
  0.7 13.4 %copy-start.1 = (bf16[512,192]{0,1:T(8,128)(2,1)S(1)}, bf16[512,192]{0,1:T(8,128)(2,1)}, u32[]{:S(2)}) copy-start(bf16[512,192]{0,1:T(8,128)(2,1)} %param.21) | copy-start | bytes 589828
  4.0 23.7 %copy-start.4 = (s32[16]{0:T(128)S(1)}, s32[16]{0:T(128)}, u32[]{:S(2)}) copy-start(s32[16]{0:T(128)} %lengths_ref.1) | copy-start | bytes 196
  4.0 10.1 %all-to-all-start = ((bf16[4,200,128]{2,1,0:T(8,128)(2,1)}), bf16[4,200,128]{2,1,0:T(8,128)(2,1)S(1)}, u32[]{:S(2)}, u32[]{:S(2)}) async-start(bf16[4,200,128]{2,1,0:T(8,128)(2,1)} %start.1), calls=%async_computation | async-start | bytes 409600 | tf_op jit(solution)/shard_map/all_to_all | solution.py:414
  15.2 32.9 %all-to-all-start.1 = ((bf16[16,160,128]{2,1,0:T(8,128)(2,1)}), bf16[16,160,128]{2,1,0:T(8,128)(2,1)S(1)}, u32[]{:S(2)}, u32[]{:S(2)}) async-start(bf16[16,160,128]{2,1,0:T(8,128)(2,1)} %get-tuple-element.9), calls=%async_computation.1 | async-start | bytes 1310720 | tf_op jit(solution)/shard_map/all_to_all | solution.py:442
  27.7 48.7 %copy-start.5 = (f32[512]{0:T(512)S(1)}, f32[512]{0:T(512)}, u32[]{:S(2)}) copy-start(f32[512]{0:T(512)} %param.26) | copy-start | bytes 6148
  28.3 52.7 %copy-start = (bf16[512,512]{1,0:T(8,128)(2,1)S(1)}, bf16[512,512]{1,0:T(8,128)(2,1)}, u32[]{:S(2)}) copy-start(bf16[512,512]{1,0:T(8,128)(2,1)} %weight_ref.1) | copy-start | bytes 1572868
  73.0 7.9 %all-to-all-start.3 = ((bf16[8,72,128]{2,1,0:T(8,128)(2,1)}), bf16[8,72,128]{2,1,0:T(8,128)(2,1)S(1)}, u32[]{:S(2)}, u32[]{:S(2)}) async-start(bf16[8,72,128]{2,1,0:T(8,128)(2,1)} %shard_map.152), calls=%async_computation.3 | async-start | bytes 294912 | tf_op jit(solution)/shard_map/all_to_all | solution.py:448
